TPU v7x, 256 devices: a 4x2x16 block of a 4x16x16 slice. The times are simulated.
256 devices in a mesh: grp: 2 (over y), sp: 32 (over z, core), tp: 4 (over x).
Axes of the slice: x: 4, y: 2, z: 16, core: 2. Of those that a mesh axis runs over, the one named last changes fastest.
The devices are a block of a 4x16x16 slice.
Arguments:
- ssm_input: bfloat16 [8192, 1024], P(('grp', 'sp'), 'tp'), parts along dimension 0, may hold values from -6 to 6
- residual_in: bfloat16 [8192, 2048], P(('grp', 'sp')), parts along dimension 0, may hold values from -4 to 4
- log_step: float32 [64], P('tp'), may hold values from -6.91 to -2.3
- decay_real: float32 [64, 64], P('tp'), may hold values from -34 to 0, as said below
- freq: float32 [64, 64], P('tp'), may hold values from 0.5 to 8
- in_real: float32 [64, 64, 16], P('tp'), may hold values from -1 to 1
- in_imag: float32 [64, 64, 16], P('tp'), may hold values from -1 to 1
- out_real: float32 [64, 16, 64], P('tp'), may hold values from -0.5 to 0.5
- out_imag: float32 [64, 16, 64], P('tp'), may hold values from -0.5 to 0.5
- skip: float32 [1024], P('tp'), may hold values from -3 to 3
- w_glu: bfloat16 [1024, 1024], replicated, may hold values from -0.1875 to 0.1875
- b_glu: float32 [1024], replicated, may hold values from -3 to 3
- w_branch: bfloat16 [1024, 2048], replicated, may hold values from -0.1875 to 0.1875
- norm_gain: float32 [2048], replicated, may hold values from 0.1 to 1.9
- w_gate: bfloat16 [2048, 5632], P('sp', 'tp'), may hold values from -0.125 to 0.125
- w_up: bfloat16 [2048, 5632], P('sp', 'tp'), may hold values from -0.125 to 0.125
- w_down: bfloat16 [5632, 2048], P('tp', 'sp'), may hold values from -0.078125 to 0.078125
Outputs:
- mixed: bfloat16 [8192, 2048], P(('grp', 'sp', 'tp')), parts along dimension 0
There are 2 independent parts, one for each index of `grp`. A program takes and returns all parts, laid end to end along the dimension named above; an argument that names none is the same for every part. Nothing has to cross between parts.
Inputs may be any that keep to these rules, and one draw needn't show every extreme that they name: `decay_real`: negative in every entry.
All inputs are finite; a program needn't handle non-finite values.
Results may differ from a plain program's by a relative error of at most 0.015.
Values may be sent and summed in bfloat16 or wider, within the bound.
A program may use at most 128 MiB of HBM per device.

v0:
```python
import math

import jax
import jax.numpy as jnp
from jax import lax
from jax.sharding import Mesh
from jax.sharding import PartitionSpec as P

SP = ("sp_0", "sp_1")
GRP_SP = ("grp", "sp_0", "sp_1")
GRP_SP_TP = ("grp", "sp_0", "sp_1", "tp")


EPS = 1e-06


def sent_together(arrays, axis, dim, along):
    ends, at = ([], 0)
    for a in arrays[:-1]:
        at += a.shape[along]
        ends.append(at)
    both = jnp.concatenate(arrays, axis=along)
    return tuple(jnp.split(lax.all_gather(both, axis, axis=dim, tiled=True), ends, axis=along))


def neutral_like(shard, identity):
    return jax.tree.map(
        lambda a, e: jnp.broadcast_to(jnp.asarray(e, a.dtype), a.shape), shard, identity
    )


def all_in_one(shard, axis):
    leaves = jax.tree.leaves(shard)
    turns = sorted(range(len(leaves)), key=lambda k: -leaves[k].size)
    width = (1, *leaves[turns[0]].shape)[-1]
    lines = [
        jnp.pad(leaves[k].reshape(-1), (0, -leaves[k].size % width)).reshape(-1, width)
        for k in turns
    ]
    both, at, found = (lax.all_gather(jnp.concatenate(lines), axis), 0, {})
    for k, line in zip(turns, lines):
        piece = both[:, at : at + len(line)].reshape(len(both), -1)
        found[k] = piece[:, : leaves[k].size].reshape(-1, *leaves[k].shape)
        at += len(line)
    numbers = iter(range(len(leaves)))
    return jax.tree.map(lambda _: found[next(numbers)], shard)


def entering_2(shard, axes, combine, identity):
    before = start = neutral_like(shard, identity)
    so_far = shard
    for axis in reversed(axes):
        count, place = (lax.axis_size(axis), lax.axis_index(axis))
        pieces = all_in_one(so_far, axis)
        inside, so_far = (start, start)
        for k in range(count):
            passed = k < place
            so_far = combine(so_far, jax.tree.map(lambda part: part[k], pieces))
            inside = jax.tree.map(lambda new, old: jnp.where(passed, new, old), so_far, inside)
        before = combine(inside, before)
    return before


def sent_to_all(shard, axis):
    count = lax.axis_size(axis)
    return lax.all_to_all(
        jnp.broadcast_to(shard[None], (count, *shard.shape)), axis, 0, 0, tiled=True
    )


def in_order(pieces, dim):
    dims = list(pieces.shape[1:])
    dims[dim] *= pieces.shape[0]
    return jnp.moveaxis(pieces, 0, dim).reshape(dims)


def gather_directly(shard, axis, dim):
    pieces = sent_to_all(shard, axis)
    return in_order(pieces, dim)


def cut_along(shard, dim, count):
    dims = shard.shape
    pieces = shard.reshape(*dims[:dim], count, dims[dim] // count, *dims[dim + 1 :])
    return jnp.moveaxis(pieces, dim, 0)


def summed_on_arrival(shard, axis, dim):
    pieces = cut_along(shard, dim, lax.axis_size(axis))
    arrived = lax.all_to_all(pieces, axis, split_axis=0, concat_axis=0, tiled=True)
    return arrived.astype(jnp.float32).sum(axis=0)


def discretize(log_step, decay_real, freq, in_real, in_imag):
    step_size = jnp.exp(log_step)[:, None]
    magnitude = jnp.exp(decay_real * step_size)
    abar_re = magnitude * jnp.cos(freq * step_size)
    abar_im = magnitude * jnp.sin(freq * step_size)
    denominator = decay_real * decay_real + freq * freq
    less_re = abar_re - 1.0
    hold_re = ((less_re * decay_real + abar_im * freq) / denominator)[..., None]
    hold_im = ((abar_im * decay_real - less_re * freq) / denominator)[..., None]
    bbar_re = hold_re * in_real - hold_im * in_imag
    bbar_im = hold_re * in_imag + hold_im * in_real
    return (step_size, abar_re, abar_im, bbar_re, bbar_im)


def powers(decay_real, freq, step_size, length):
    steps_up = (jnp.arange(length, dtype=jnp.int32) + 1).astype(jnp.float32)[:, None, None]
    magnitude = jnp.exp((decay_real * step_size)[None] * steps_up)
    phase = (freq * step_size)[None] * steps_up
    return (magnitude * jnp.cos(phase), magnitude * jnp.sin(phase))


def compose(earlier, later):
    a1r, a1i, b1r, b1i = earlier
    a2r, a2i, b2r, b2i = later
    return (
        a2r * a1r - a2i * a1i,
        a2r * a1i + a2i * a1r,
        a2r * b1r - a2i * b1i + b2r,
        a2r * b1i + a2i * b1r + b2i,
    )


def local_states(inputs, decay_real, freq, step_size, bbar_re, bbar_im):
    highest = lax.Precision.DEFAULT
    tok_rows, group_count, unused = inputs.shape
    lanes = group_count * decay_real.shape[1]
    drive_re = jnp.einsum("lgm,gpm->lgp", inputs, bbar_re, precision=highest).reshape(
        tok_rows, lanes
    )
    drive_im = jnp.einsum("lgm,gpm->lgp", inputs, bbar_im, precision=highest).reshape(
        tok_rows, lanes
    )
    span = math.gcd(tok_rows, 16)
    spans = tok_rows // span
    rate = (decay_real * step_size).reshape(lanes)
    turn = (freq * step_size).reshape(lanes)
    later = jnp.arange(span, dtype=jnp.int32)[:, None]
    earlier = jnp.arange(span, dtype=jnp.int32)[None, :]
    lag = (later - earlier).astype(jnp.float32)
    causal = (later >= earlier)[..., None]
    lag_pos = jnp.maximum(lag, 0.0)[..., None]
    table_mag = jnp.exp(rate[None, None] * lag_pos)
    table_re = jnp.where(causal, table_mag * jnp.cos(turn[None, None] * lag_pos), 0.0)
    table_im = jnp.where(causal, table_mag * jnp.sin(turn[None, None] * lag_pos), 0.0)
    block_re = drive_re.reshape(spans, 1, span, lanes)
    block_im = drive_im.reshape(spans, 1, span, lanes)
    inner_re = jnp.sum(table_re[None] * block_re - table_im[None] * block_im, axis=2)
    inner_im = jnp.sum(table_re[None] * block_im + table_im[None] * block_re, axis=2)
    steps_up = (jnp.arange(span, dtype=jnp.int32) + 1).astype(jnp.float32)[:, None]
    pow_mag = jnp.exp(rate[None] * steps_up)
    pow_re = pow_mag * jnp.cos(turn[None] * steps_up)
    pow_im = pow_mag * jnp.sin(turn[None] * steps_up)
    span_re = pow_re[-1]
    span_im = pow_im[-1]

    def carry_step(entering, ends):
        next_re = span_re * entering[0] - span_im * entering[1] + ends[0]
        next_im = span_re * entering[1] + span_im * entering[0] + ends[1]
        return ((next_re, next_im), entering)

    zeros = jnp.zeros((lanes,), jnp.float32)
    unused_carry, entering = lax.scan(
        carry_step, (zeros, zeros), (inner_re[:, -1], inner_im[:, -1])
    )
    state_re = inner_re + pow_re[None] * entering[0][:, None] - pow_im[None] * entering[1][:, None]
    state_im = inner_im + pow_re[None] * entering[1][:, None] + pow_im[None] * entering[0][:, None]
    shape = (tok_rows, group_count, decay_real.shape[1])
    return (state_re.reshape(shape), state_im.reshape(shape))


def readout(state_re, state_im, out_real, out_imag, skip_mat, inputs):
    highest = lax.Precision.DEFAULT
    values = (
        jnp.einsum("lgp,gmp->lgm", state_re, out_real, precision=highest)
        - jnp.einsum("lgp,gmp->lgm", state_im, out_imag, precision=highest)
        + skip_mat[None] * inputs
    )
    values = jax.nn.gelu(values)
    return values.reshape(values.shape[0], -1).astype(jnp.bfloat16)


def row_norm(stream, norm_gain):
    scale_rows = lax.rsqrt(jnp.mean(stream * stream, axis=-1, keepdims=True) + EPS)
    return (stream * scale_rows * norm_gain).astype(jnp.bfloat16)


def per_device(
    ssm_input,
    residual_in,
    log_step,
    decay_real,
    freq,
    in_real,
    in_imag,
    out_real,
    out_imag,
    skip,
    w_glu,
    b_glu,
    w_branch,
    norm_gain,
    w_gate,
    w_up,
    w_down,
):
    tok_rows, width_local = ssm_input.shape
    group_count = log_step.shape[0]
    group_size = in_real.shape[2]
    tp_count = lax.axis_size("tp")
    tp_index = lax.axis_index("tp")
    own_rows = tok_rows // tp_count
    gate_whole, up_whole = sent_together((w_gate, w_up), SP, 0, 1)
    step_size, abar_re, abar_im, bbar_re, bbar_im = discretize(
        log_step, decay_real, freq, in_real, in_imag
    )
    pow_re, pow_im = powers(decay_real, freq, step_size, tok_rows)
    inputs = ssm_input.astype(jnp.float32).reshape(tok_rows, group_count, group_size)
    local_re, local_im = local_states(inputs, decay_real, freq, step_size, bbar_re, bbar_im)
    identity = (
        jnp.ones_like(abar_re),
        jnp.zeros_like(abar_re),
        jnp.zeros_like(abar_re),
        jnp.zeros_like(abar_re),
    )
    carried = entering_2(
        (pow_re[-1], pow_im[-1], local_re[-1], local_im[-1]), SP, compose, identity
    )
    state_re = local_re + pow_re * carried[2][None] - pow_im * carried[3][None]
    state_im = local_im + pow_re * carried[3][None] + pow_im * carried[2][None]
    mixer_out = readout(
        state_re, state_im, out_real, out_imag, skip.reshape(group_count, group_size), inputs
    )
    mixer_rows = lax.all_to_all(mixer_out, "tp", split_axis=0, concat_axis=1, tiled=True)
    glu_pre = jnp.dot(mixer_rows, w_glu, preferred_element_type=jnp.float32) + b_glu
    gated = (mixer_rows.astype(jnp.float32) * jax.nn.sigmoid(glu_pre)).astype(jnp.bfloat16)
    residual_own = lax.dynamic_slice_in_dim(residual_in, tp_index * own_rows, own_rows, 0)
    stream = residual_own.astype(jnp.float32) + jnp.dot(
        gated, w_branch, preferred_element_type=jnp.float32
    )
    normed = row_norm(stream, norm_gain)
    normed_all = gather_directly(normed, "tp", 0)
    gate_sum = jnp.dot(normed_all, gate_whole, preferred_element_type=jnp.float32)
    up_sum = jnp.dot(normed_all, up_whole, preferred_element_type=jnp.float32)
    hidden = (jax.nn.silu(gate_sum) * up_sum).astype(jnp.bfloat16)
    down_whole = lax.all_gather(w_down, SP, axis=1, tiled=True)
    summed = summed_on_arrival(
        jnp.dot(hidden, down_whole, preferred_element_type=jnp.float32).astype(jnp.bfloat16),
        "tp",
        0,
    )
    return (stream + summed).astype(jnp.bfloat16)


def solution(mesh):
    torus = Mesh(
        mesh.devices.reshape(mesh.shape["grp"], 16, 2, mesh.shape["tp"]),
        ("grp", "sp_0", "sp_1", "tp"),
    )
    in_specs = (
        P(GRP_SP, "tp"),
        P(GRP_SP, None),
        P("tp"),
        P("tp", None),
        P("tp", None),
        P("tp", None, None),
        P("tp", None, None),
        P("tp", None, None),
        P("tp", None, None),
        P("tp"),
        P(),
        P(),
        P(),
        P(),
        P(SP, "tp"),
        P(SP, "tp"),
        P("tp", SP),
    )
    out_specs = P(GRP_SP_TP, None)
    return jax.shard_map(
        per_device, mesh=torus, in_specs=in_specs, out_specs=out_specs, check_vma=False
    )
```

profile of v0, /device:TPU:40, one launch (start us, length us, event | category | flops | bytes accessed | tf_op | source)
XLA Modules:
  0.0 208.6 jit_solution(3152876637672829027)
XLA Ops:
  6.6 0.0 all-gather.5.cloned.1.call-start
  6.6 1.9 pad_maximum_fusion
  8.5 0.1 all-gather.5.cloned.1.call-update
  8.5 0.1 all-gather.7.cloned.1.call-start
  8.6 0.7 all-gather.7.cloned.1.call-update
  9.4 0.7 exp.36
  10.0 0.8 fusion.68
  10.9 0.1 mul.856
  10.9 0.1 mul.861
  11.0 0.9 copy.43
  12.0 5.8 %fusion.19 = (f32[16,16,1024]{2,1,0:T(8,128)}, f32[16,16,1024]{2,1,0:T(8,128)}) fusion(f32[1024]{0:T(1024)S(1)} %mul.861, f32[16,16]{1,0:T(8,128)S(1)} %convert_maximum_fusion, f32[1024]{0:T(1024)S(1)} %mul.856, pred[16,16]{1,0:T(8,128)(4,1)S(1)} %iota_compare_fusion), kind=kLoop, calls=%fused_computation.33 | loop fusion | flops 1572864 | bytes 2106624 | tf_op jit(solution)/shard_map/jit(_where)/select_n | solution.py:146
  17.8 2.0 convolution_bitcast_fusion.1
  19.8 2.0 convolution_bitcast_fusion
  21.8 1.5 copy.44
  23.4 1.1 mul.878
  24.5 1.5 copy.45
  26.1 1.1 mul.885
  27.2 6.3 %add_reduce_fusion = (f32[8,16,1024]{2,1,0:T(8,128)S(1)}, f32[8,16,1024]{2,1,0:T(8,128)S(1)}) fusion(f32[8,16,1024]{2,1,0:T(8,128)} %mul.885, f32[16,16,1024]{2,1,0:T(8,128)} %get-tuple-element.125, f32[8,16,1024]{2,1,0:T(8,128)} %mul.878, f32[16,16,1024]{2,1,0:T(8,128)} %get-tuple-element.124), kind=kLoop, calls=%fused_computation.6 | loop fusion | flops 16515072 | bytes 4194304 | tf_op jit(solution)/shard_map/reduce_sum | solution.py:151
  33.6 0.3 fusion.55
  34.0 12.5 %while.17 = (s32[]{:T(128)}, f32[1024]{0:T(1024)S(1)}, f32[1024]{0:T(1024)S(1)}, f32[8,1024]{1,0:T(8,128)S(1)}, f32[8,1024]{1,0:T(8,128)}, /*index=5*/f32[1024]{...) while((s32[]{:T(128)}, f32[1024]{0:T(1024)S(1)}, ...), condition=%wide.region_3.4_spmd.clone, body=%wide.region_2.3_spmd.clone.sunk | while | flops 10243 | bytes 90243 | solution.py:165
  34.0 0.1 dynamic_update_slice.11
  34.2 1.4 dynamic_update_slice.12
  35.6 0.1 dynamic_update_slice.11
  35.7 1.4 dynamic_update_slice.12
  37.2 0.1 dynamic_update_slice.11
  37.3 1.4 dynamic_update_slice.12
  38.7 0.1 dynamic_update_slice.11
  38.9 1.4 dynamic_update_slice.12
  40.3 0.1 dynamic_update_slice.11
  40.4 1.4 dynamic_update_slice.12
  41.9 0.1 dynamic_update_slice.11
  42.0 1.4 dynamic_update_slice.12
  43.4 0.1 dynamic_update_slice.11
  43.5 1.4 dynamic_update_slice.12
  45.0 0.1 dynamic_update_slice.11
  45.1 1.4 dynamic_update_slice.12
  46.5 1.9 multiply_add_fusion.1
  48.4 1.3 add.447
  49.8 0.0 copy-start.3
  49.8 2.3 %sub.173 = f32[128,16,64]{2,1,0:T(8,128)} reshape(f32[8,16,1024]{2,1,0:T(8,128)} %get-tuple-element.118) | data formatting | bytes 1048576 | tf_op jit(solution)/shard_map/sub | solution.py:168
  52.1 0.1 mul.1006
  52.2 0.7 slice_bitcast_fusion.1
  52.9 3.9 %fusion.22 = (f32[128,16,64]{2,1,0:T(8,128)S(1)}, f32[128,16,64]{2,1,0:T(8,128)S(1)}) fusion(f32[16,64]{1,0:T(8,128)S(1)} %get-tuple-element.133, f32[128]{0:T(128)S(1)} %add_convert_fusion.1, f32[16,64]{1,0:T(8,128)S(1)} %get-tuple-element.132), kind=kLoop, calls=%fused_computation.36 | loop fusion | flops 524288 | bytes 1057280 | tf_op jit(solution)/shard_map/mul | solution.py:112
  56.8 1.9 all-gather
  58.8 54.9 %all-gather.1 = f32[1024,64]{1,0:T(8,128)S(1)} all-gather(f32[64,64]{1,0:T(8,128)S(1)} %pad_maximum_fusion.2), channel_id=3, replica_groups=mesh['grp'=2,'sp_0'=16,'sp_1'=2,'tp'=4] {'sp_0'}, dimensions={0}, use_global_device_ids=true | all-gather | bytes 278528 | tf_op jit(solution)/shard_map/all_gather | solution.py:40
  113.6 0.1 add_bitcast_fusion.1
  113.7 0.0 copy-start.2
  113.7 6.7 %multiply_add_fusion = (bf16[128,16,64]{2,1,0:T(8,128)(2,1)S(1)}, bf16[128,16,64]{2,1,0:T(8,128)(2,1)S(1)}) fusion(f32[128,16,64]{2,1,0:T(8,128)S(1)} %add.447, f32[16,64]{1,0:T(8,128)S(1)} %add_bitcast_fusion, f32[16,64]{1,0:T(8,128)S(1)} %get-tuple-element.108, f32[16,64]{1,0:T(8,128)S(1)} %get-tuple-element.133, f32[128]{0:T(128)S(1)} %add_convert_fusion.1, ...), kind=kLoop, calls=%fused_computation.42 | loop fusion | flops 1835008 | bytes 1589760 | tf_op jit(solution)/shard_map/add | solution.py:232
  120.5 0.4 fusion.25
  120.8 1.3 fusion.44
  122.2 0.2 convert_element_type.64
  122.3 0.8 copy.48
  123.1 4.5 %all-to-all-start = ((bf16[4,32,256]{2,1,0:T(8,128)(2,1)}), bf16[4,32,256]{2,1,0:T(8,128)(2,1)S(1)}, u32[]{:S(2)}, u32[]{:S(2)}) async-start(bf16[4,32,256]{2,1,0:T(8,128)(2,1)} %copy.48), calls=%async_computation | async-start | bytes 131072 | tf_op jit(solution)/shard_map/all_to_all | solution.py:236
  127.6 5.6 %all-to-all-done = bf16[4,32,256]{2,1,0:T(8,128)(2,1)S(1)} async-done(((bf16[4,32,256]{2,1,0:T(8,128)(2,1)}), bf16[4,32,256]{2,1,0:T(8,128)(2,1)S(1)}, u32[]{:S(2)}, u32[]{:S(2)}) %all-to-all-start) | async-done | bytes 65568 | tf_op jit(solution)/shard_map/all_to_all | solution.py:236
  133.3 0.0 copy-done
  133.3 3.6 %multiply_reduce_fusion = (f32[32]{0:T(128)S(1)}, f32[32,2048]{1,0:T(8,128)S(1)}) fusion(bf16[1024,2048]{1,0:T(8,128)(2,1)} %param.31, bf16[32,1024]{1,0:T(8,128)(2,1)S(1)} %bitcast.174, bf16[1024,1024]{1,0:T(8,128)(2,1)S(1)} %copy-done, f32[1024]{0:T(1024)S(1)} %copy-done.3, bf16[128,2048]{1,0:T(8,128)(2,1)} %param.20, s32[]{:T(128)S(6)} %select_n.296), kind=kOutput, calls=%fused_computation.57 | convolution fusion | flops 201818080 | bytes 6819972 | tf_op jit(solution)/shard_map/dot_general | solution.py:240
  136.9 0.1 multiply_convert_fusion
  137.0 10.5 %all_to_all.26 = bf16[4,32,2048]{2,1,0:T(8,128)(2,1)S(1)} all-to-all(bf16[4,32,2048]{2,1,0:T(8,128)(2,1)S(1)} %broadcast_in_dim.32), channel_id=1, replica_groups=mesh['grp'=2,'sp_0'=16,'sp_1'=2,'tp'=4] {'tp'}, dimensions={0} | all-to-all | bytes 1048576 | tf_op jit(solution)/shard_map/all_to_all | solution.py:66
  147.6 4.6 %fusion.2 = f32[128,1408]{1,0:T(8,128)} fusion(bf16[128,2048]{1,0:T(8,128)(2,1)S(1)} %bitcast.167, bf16[2048,2816]{1,0:T(8,128)(2,1)} %all-gather.5.cloned.1.call-done), kind=kOutput, calls=%fused_computation.10 | convolution fusion | flops 738197504 | bytes 7012352 | tf_op jit(solution)/shard_map/dot_general | solution.py:245
  152.1 27.5 %all-gather.7.cloned.1.call-done = bf16[1408,2048]{0,1:T(8,128)(2,1)} async-done(((bf16[1408,64]{0,1:T(8,128)(2,1)}), bf16[1408,2048]{0,1:T(8,128)(2,1)}) %all-gather.7.cloned.1.call-update) | async-done | bytes 5767184 | tf_op jit(solution)/shard_map/all_gather | solution.py:248
  179.6 7.4 %convolution_convert_fusion = bf16[128,2048]{1,0:T(8,128)(2,1)S(1)} fusion(bf16[1408,2048]{0,1:T(8,128)(2,1)} %all-gather.7.cloned.1.call-done, bf16[128,2048]{1,0:T(8,128)(2,1)S(1)} %bitcast.168, bf16[2048,2816]{1,0:T(8,128)(2,1)} %all-gather.5.cloned.1.call-done, f32[128,1408]{1,0:T(8,128)} %fusion.2), kind=kOutput, calls=%fused_computation.14 | convolution fusion | flops 1477738496 | bytes 13303808 | tf_op jit(solution)/shard_map/dot_general | solution.py:250
  187.0 14.0 %all_to_all.27 = bf16[4,32,2048]{2,1,0:T(8,128)(2,1)S(1)} all-to-all(bf16[4,32,2048]{2,1,0:T(8,128)(2,1)S(1)} %bitcast.169), channel_id=1, replica_groups=mesh['grp'=2,'sp_0'=16,'sp_1'=2,'tp'=4] {'tp'}, dimensions={0} | all-to-all | bytes 1048576 | tf_op jit(solution)/shard_map/all_to_all | solution.py:90
  201.0 0.1 convert_reduce_fusion
  201.1 0.7 add_convert_fusion
  (55 shorter events, 0.5 us)
Async XLA Ops:
  6.5 126.7 %copy-start = (bf16[1024,1024]{1,0:T(8,128)(2,1)S(1)}, bf16[1024,1024]{1,0:T(8,128)(2,1)}, u32[]{:S(2)}) copy-start(bf16[1024,1024]{1,0:T(8,128)(2,1)} %param.29) | copy-start | bytes 6291460
  6.6 141.0 %all-gather.5.cloned.1.call-start = ((), (), s32[]{:S(2)}) async-start(), calls=%async_computation.3 | async-start | bytes 11894784 | tf_op jit(solution)/shard_map/all_gather | solution.py:23
  8.5 171.0 %all-gather.7.cloned.1.call-start = ((), (), s32[]{:S(2)}) async-start(), calls=%async_computation.4 | async-start | bytes 5947392 | tf_op jit(solution)/shard_map/all_gather | solution.py:248
  27.2 24.9 %copy-start.4 = (f32[256]{0:T(256)S(1)}, f32[256]{0:T(256)}, u32[]{:S(2)}) copy-start(f32[256]{0:T(256)} %param.28) | copy-start | bytes 3076
  46.5 74.0 %copy-start.1 = (f32[16,16,64]{2,1,0:T(8,128)S(1)}, f32[16,16,64]{2,1,0:T(8,128)}, u32[]{:S(2)}) copy-start(f32[16,16,64]{2,1,0:T(8,128)} %param.26) | copy-start | bytes 196612
  49.8 83.5 %copy-start.3 = (f32[1024]{0:T(1024)S(1)}, f32[1024]{0:T(1024)}, u32[]{:S(2)}) copy-start(f32[1024]{0:T(1024)} %param.30) | copy-start | bytes 12292
  113.7 23.1 %copy-start.2 = (f32[2048]{0:T(1024)S(1)}, f32[2048]{0:T(1024)}, u32[]{:S(2)}) copy-start(f32[2048]{0:T(1024)} %param.32) | copy-start | bytes 24580
  123.1 10.1 %all-to-all-start = ((bf16[4,32,256]{2,1,0:T(8,128)(2,1)}), bf16[4,32,256]{2,1,0:T(8,128)(2,1)S(1)}, u32[]{:S(2)}, u32[]{:S(2)}) async-start(bf16[4,32,256]{2,1,0:T(8,128)(2,1)} %copy.48), calls=%async_computation | async-start | bytes 131072 | tf_op jit(solution)/shard_map/all_to_all | solution.py:236
Sparse Core Ops, SparseCore 0:
  9.2 99.0 all-gather.4
  110.2 69.3 all-gather.6
where the time goes:
time: 210 us; the launch traced here: 209 us
  blocking collectives  81.3 us (39%)
  waiting for transfers between devices  33.9 us (16%)
  other arithmetic  28.9 us (14%)
  local copies, waits for them, and re-layouts  24.7 us (12%)
  matrix products  21.3 us (10%)
  between operations  13.7 us (7%)
  starting transfers between devices  4.57 us (2%)
    all_gather x2, blocking collectives, all_in_one(): both, at, found = (lax.all_gather(jnp.concatenate(lines), axis), 0, {})  56.8 us
    all_gather x1, waiting for transfers between devices, per_device(): down_whole = lax.all_gather(w_down, SP, axis=1, tiled=True)  27.5 us
    all_to_all x1, blocking collectives, summed_on_arrival(): lax.all_to_all(pieces, axis, split_axis=0, concat_axis=0, tiled=True)  14 us
    dynamic_update_slice x16, local copies, waits for them, and re-layouts, local_states(): lax.scan(carry_step, (zeros, zeros), (inner_re[:, -1], inner_im[:, -1]))  12.1 us
    all_to_all x1, blocking collectives, sent_to_all(): lax.all_to_all(jnp.broadcast_to(shard[None], (count, *shard.shape)), axis...  10.5 us
    dot_general x1, matrix products, per_device(): jnp.dot(hidden, down_whole, preferred_element_type=jnp.float32)  7.42 us
    add x1, other arithmetic, per_device(): state_im = local_im + pow_re * carried[3][None] + pow_im * carried[2][None]  6.71 us
    reduce_sum x1, other arithmetic, local_states(): jnp.sum(table_re[None] * block_im + table_im[None] * block_re, axis=2)  6.35 us
  transfers between devices with their start and end apart: 3, of which 2 were waited for; matrix products, arithmetic and copies ran while one was open for 31% of the time, Pallas kernels for 0%

commit v1 on v0

v1 whole, which is shorter than its diff:
```python
import functools

import jax
import jax.numpy as jnp
from jax import lax
from jax.experimental import pallas as pl
from jax.experimental.pallas import tpu as pltpu
from jax.sharding import Mesh
from jax.sharding import PartitionSpec as P

SP = ("sp_0", "sp_1")
GRP_SP = ("grp", "sp_0", "sp_1")
GRP_SP_TP = ("grp", "sp_0", "sp_1", "tp")
EPS = 1e-06
LANES = 128
SPAN = 16
ROWS8 = 8
BF = jnp.bfloat16
F32 = jnp.float32
MESH = pl.DeviceIdType.MESH


def mod(a, n):
    return lax.rem(a + 8 * n, n)


def cmul(ar, ai, br, bi):
    return ar * br - ai * bi, ar * bi + ai * br


def dot(a, b):
    return jnp.dot(a, b, preferred_element_type=F32)


def dot_t(a, b):
    return lax.dot_general(a, b, (((1,), (1,)), ((), ())), preferred_element_type=F32)


def tile(v, k):
    return v[:, k * LANES : (k + 1) * LANES]


def swap_halves(v, forward):
    rows, width = v.shape
    half = width // LANES // 2
    low = lax.broadcasted_iota(jnp.int32, (rows, LANES), 1) < LANES // 2
    first, second = [], []
    for k in range(half):
        one, two = (tile(v, 2 * k), tile(v, 2 * k + 1)) if forward else (tile(v, k), tile(v, half + k))
        first.append(jnp.where(low, one, pltpu.roll(two, LANES // 2, 1)))
        second.append(jnp.where(low, pltpu.roll(one, LANES // 2, 1), two))
    if forward:
        return jnp.concatenate(first + second, axis=1)
    return jnp.concatenate([t for pair in zip(first, second) for t in pair], axis=1)


def kernel(
    dims,
    u_ref, ls_ref, dr_ref, fq_ref, inr_ref, ini_ref, our_ref, oui_ref, skip_ref, bglu_ref, gain_ref,
    resid_hbm, wglu_hbm, wbr_hbm, wg_hbm, wu_hbm, wd_hbm,
    out_ref,
    wglu, wbr, resid, w, tab_b, tab_c, drive, states, est, gst, mo, mrecv, act, stream, own, part, sbuf, rbuf,
    cp_sem, st_send, st_recv, e_send, e_recv, g_send, g_recv, m_send, m_recv,
    xf_send, xf_recv, xh_send, xh_recv, p_send, p_recv, ag_send, ag_recv, rs_send, rs_recv,
):
    n_z, n_x, tiles, slots = dims
    quads = n_z // n_x
    z, c, x = lax.axis_index("sp_0"), lax.axis_index("sp_1"), lax.axis_index("tp")
    zq = lax.div(z, n_x)
    right, left = {"sp_0": mod(z + 1, n_z)}, {"sp_0": mod(z - 1, n_z)}
    other = {"sp_1": 1 - c}
    tok, width = u_ref.shape
    groups, lanes_state = dr_ref.shape
    n_state = groups * lanes_state
    half_z = n_z // 2
    own_rows, d = stream.shape
    d_half = d // 2
    d_block = d_half // n_z
    ff_pad = slots * LANES

    barrier = pltpu.get_barrier_semaphore()

    def greet(k, unused):
        pl.semaphore_signal(barrier, inc=1, device_id={"sp_0": mod(z + k, n_z)}, device_id_type=MESH)
        return unused

    lax.fori_loop(1, n_z, greet, 0)
    for k in range(1, n_x):
        pl.semaphore_signal(barrier, inc=1, device_id={"tp": mod(x + k, n_x)}, device_id_type=MESH)
    pl.semaphore_signal(barrier, inc=1, device_id=other, device_id_type=MESH)

    local = [
        pltpu.make_async_copy(wglu_hbm, wglu, cp_sem.at[0]),
        pltpu.make_async_copy(wbr_hbm, wbr, cp_sem.at[1]),
        pltpu.make_async_copy(resid_hbm.at[pl.ds(pl.multiple_of(x * own_rows, own_rows), own_rows)], resid, cp_sem.at[2]),
    ]
    for copy in local:
        copy.start()

    diag = lax.broadcasted_iota(jnp.int32, (groups, groups), 0) == lax.broadcasted_iota(jnp.int32, (groups, groups), 1)
    step = jnp.sum(jnp.where(diag, jnp.broadcast_to(jnp.exp(ls_ref[...]), (groups, groups)), 0.0), axis=1, keepdims=True)
    dr, fq = dr_ref[...], fq_ref[...]
    mag = jnp.exp(dr * step)
    abar_re, abar_im = mag * jnp.cos(fq * step), mag * jnp.sin(fq * step)
    denominator = dr * dr + fq * fq
    less_re = abar_re - 1.0
    hold_re = (less_re * dr + abar_im * fq) / denominator
    hold_im = (abar_im * dr - less_re * fq) / denominator

    def row_form(v):
        twice = jnp.concatenate([v, v], axis=1)
        row = lax.broadcasted_iota(jnp.int32, (groups, LANES), 0)
        lane = lax.broadcasted_iota(jnp.int32, (groups, LANES), 1)
        pieces = []
        for k in range(n_state // LANES):
            keep = row == 2 * k + lax.div(lane, lanes_state)
            pieces.append(jnp.sum(jnp.where(keep, twice, 0.0), axis=0, keepdims=True))
        return jnp.concatenate(pieces, axis=1)

    a_re, a_im = row_form(abar_re), row_form(abar_im)
    h_re, h_im = row_form(hold_re), row_form(hold_im)

    group_size = width // groups
    pair_rows = 2 * group_size
    row = lax.broadcasted_iota(jnp.int32, (pair_rows, LANES), 0)
    lane = lax.broadcasted_iota(jnp.int32, (pair_rows, LANES), 1)
    keep = lax.div(row, group_size) == lax.div(lane, lanes_state)

    tab_b[...] = jnp.zeros_like(tab_b)
    tab_c[...] = jnp.zeros_like(tab_c)

    def put(table, k, col, value):
        table[k * pair_rows : (k + 1) * pair_rows, col + k * LANES : col + (k + 1) * LANES] = jnp.where(keep, value, 0.0).astype(BF)

    def twice_of(ref, k):
        v = ref[k * pair_rows : (k + 1) * pair_rows, :]
        return jnp.concatenate([v, v], axis=1)

    for k in range(n_state // LANES):
        hr, hi = tile(h_re, k), tile(h_im, k)
        ir, ii = twice_of(inr_ref, k), twice_of(ini_ref, k)
        put(tab_b, k, 0, hr * ir - hi * ii)
        put(tab_b, k, n_state, hr * ii + hi * ir)
        put(tab_c, k, 0, twice_of(our_ref, k))
        put(tab_c, k, n_state, -twice_of(oui_ref, k))

    to_row = lax.broadcasted_iota(jnp.int32, (tok, tok), 0)
    to_col = lax.broadcasted_iota(jnp.int32, (tok, tok), 1)
    order = (to_col == lax.rem(to_row, ROWS8) * SPAN + lax.div(to_row, ROWS8)).astype(F32).astype(BF)
    back = (to_row == lax.rem(to_col, ROWS8) * SPAN + lax.div(to_col, ROWS8)).astype(F32).astype(BF)
    u_perm = dot(order, u_ref[...])
    drive[...] = dot(u_perm.astype(BF), tab_b[...])

    ar, ai = jnp.broadcast_to(a_re, (ROWS8, n_state)), jnp.broadcast_to(a_im, (ROWS8, n_state))
    s_re = drive[0:ROWS8, 0:n_state]
    s_im = drive[0:ROWS8, n_state:]
    for j in range(1, SPAN):
        at = slice(j * ROWS8, (j + 1) * ROWS8)
        p_re, p_im = cmul(ar, ai, s_re, s_im)
        s_re = p_re + drive[at, 0:n_state]
        s_im = p_im + drive[at, n_state:]
        drive[at, 0:n_state] = s_re
        drive[at, n_state:] = s_im

    pw = [(ar, ai)]
    for _ in range(8):
        pw.append(cmul(*pw[-1], *pw[-1]))
    chunk = lax.broadcasted_iota(jnp.int32, (ROWS8, n_state), 0)

    def shifted(v, by):
        return jnp.where(chunk >= by, pltpu.roll(v, by, 0), 0.0)

    i_re, i_im = s_re, s_im
    for level, by in ((4, 1), (5, 2), (6, 4)):
        q_re, q_im = cmul(*pw[level], shifted(i_re, by), shifted(i_im, by))
        i_re, i_im = i_re + q_re, i_im + q_im
    before_re, before_im = shifted(i_re, 1), shifted(i_im, 1)
    end_re, end_im = i_re[ROWS8 - 1 :, :], i_im[ROWS8 - 1 :, :]
    est[0, 0:1, :] = end_re
    est[0, 1:2, :] = end_im
    a128 = (pw[7][0][0:1], pw[7][1][0:1])
    a256 = (pw[8][0][0:1], pw[8][1][0:1])

    for s in range(slots):
        if s * quads + quads - 1 >= tiles:

            @pl.when(s * quads + zq >= tiles)
            def _():
                for m in range(3):
                    at = (m * slots + s) * LANES
                    w[:, :, at : at + LANES] = jnp.zeros((2, d_half, LANES), BF)

    pl.semaphore_wait(barrier, n_z - 1 + n_x - 1 + 1)

    e_copy = pltpu.make_async_remote_copy(
        src_ref=est.at[0], dst_ref=est.at[1], send_sem=e_send.at[0], recv_sem=e_recv.at[0], device_id=other, device_id_type=MESH
    )
    e_copy.start()
    e_copy.wait_recv()
    oth_re, oth_im = est[1, 0:1, :], est[1, 1:2, :]
    first = c == 0
    e0_re, e0_im = jnp.where(first, end_re, oth_re), jnp.where(first, end_im, oth_im)
    e1_re, e1_im = jnp.where(first, oth_re, end_re), jnp.where(first, oth_im, end_im)
    g_re, g_im = cmul(*a128, e0_re, e0_im)
    est[2, 0:1, :] = g_re + e1_re
    est[2, 1:2, :] = g_im + e1_im

    def g_copy(to):
        return pltpu.make_async_remote_copy(
            src_ref=est.at[2], dst_ref=gst.at[z], send_sem=g_send.at[to], recv_sem=g_recv.at[z],
            device_id={"sp_0": to}, device_id_type=MESH,
        )

    def g_start(to, unused):
        g_copy(to).start()
        return unused

    lax.fori_loop(z + 1, n_z, g_start, 0)

    sources = (wg_hbm, wu_hbm, wd_hbm)

    def w_at(core, rows, m, s):
        return w.at[core, rows, pl.ds(pl.multiple_of((m * slots + s) * LANES, LANES), LANES)]

    z_rows = pl.ds(pl.multiple_of(z * d_block, d_block), d_block)
    all_rows = pl.ds(0, d_half)

    def st_place(j):
        s = lax.div(j, quads)
        return s, lax.rem(j, quads) * n_x + mod(x - s, n_x)

    def st_copy(m, j, s, to):
        src = sources[m].at[:, pl.ds(pl.multiple_of(j * LANES, LANES), LANES)]
        return pltpu.make_async_remote_copy(
            src_ref=src, dst_ref=w_at(c, z_rows, m, s), send_sem=st_send.at[m, j], recv_sem=st_recv.at[m],
            device_id={"sp_0": to}, device_id_type=MESH,
        )

    for m in range(3):

        def st_start(j, unused, m=m):
            s, to = st_place(j)

            @pl.when(to != z)
            def _():
                st_copy(m, j, s, to).start()

            @pl.when(to == z)
            def _():
                src = sources[m].at[:, pl.ds(pl.multiple_of(j * LANES, LANES), LANES)]
                pltpu.make_async_copy(src, w_at(c, z_rows, m, s), st_recv.at[m]).start()

            return unused

        lax.fori_loop(0, tiles, st_start, 0)

    def add_state(frm, carry):
        g_got = pltpu.make_async_remote_copy(
            src_ref=est.at[2], dst_ref=gst.at[frm], send_sem=g_send.at[frm], recv_sem=g_recv.at[frm],
            device_id={"sp_0": frm}, device_id_type=MESH,
        )
        g_got.wait_recv()
        n_re, n_im = cmul(*a256, *carry)
        return n_re + gst[frm, 0:1, :], n_im + gst[frm, 1:2, :]

    zero_row = jnp.zeros((1, n_state), F32)
    in_re, in_im = lax.fori_loop(0, z, add_state, (zero_row, zero_row))
    t_re, t_im = cmul(*a128, in_re, in_im)
    in_re, in_im = jnp.where(first, in_re, t_re + oth_re), jnp.where(first, in_im, t_im + oth_im)

    one, nil = jnp.ones((ROWS8, n_state), F32), jnp.zeros((ROWS8, n_state), F32)
    r_re, r_im = one, nil
    for level, bit in ((4, 1), (5, 2), (6, 4)):
        has = lax.rem(lax.div(chunk, bit), 2) == 1
        r_re, r_im = cmul(r_re, r_im, jnp.where(has, pw[level][0], one), jnp.where(has, pw[level][1], nil))
    c_re, c_im = cmul(r_re, r_im, jnp.broadcast_to(in_re, (ROWS8, n_state)), jnp.broadcast_to(in_im, (ROWS8, n_state)))
    c_re, c_im = c_re + before_re, c_im + before_im
    for jj in range(SPAN // 2):
        out_re, out_im = [], []
        for j in (2 * jj, 2 * jj + 1):
            at = slice(j * ROWS8, (j + 1) * ROWS8)
            c_re, c_im = cmul(ar, ai, c_re, c_im)
            out_re.append(drive[at, 0:n_state] + c_re)
            out_im.append(drive[at, n_state:] + c_im)
        at = slice(2 * jj * ROWS8, 2 * (jj + 1) * ROWS8)
        states[at, 0:n_state] = jnp.concatenate(out_re, axis=0).astype(BF)
        states[at, n_state:] = jnp.concatenate(out_im, axis=0).astype(BF)
    values = dot_t(states[...], tab_c[...]) + skip_ref[...] * u_perm
    cubic = 0.7978845608028654 * (values + 0.044715 * (values * values * values))
    values = values * (0.5 * (1.0 + jnp.tanh(cubic)))
    mixed = dot(back, values.astype(BF)).astype(BF)
    for k in range(n_x):
        mo[k] = mixed[k * own_rows : (k + 1) * own_rows, :]

    def m_copy(k):
        to = mod(x + k, n_x)
        return pltpu.make_async_remote_copy(
            src_ref=mo.at[to], dst_ref=mrecv.at[x], send_sem=m_send.at[k], recv_sem=m_recv.at[k],
            device_id={"tp": to}, device_id_type=MESH,
        )

    for k in range(1, n_x):
        m_copy(k).start()
    mrecv[x] = mo[x]
    for copy in local:
        copy.wait()
    for k in range(1, n_x):
        m_copy(k).wait_recv()
    rows_in = jnp.concatenate([mrecv[k] for k in range(n_x)], axis=1)
    glu = dot(rows_in, wglu[...]) + bglu_ref[...]
    gated = (rows_in.astype(F32) / (1.0 + jnp.exp(-glu))).astype(BF)
    st = resid[...].astype(F32) + dot(gated, wbr[...])
    stream[...] = st
    scale = lax.rsqrt(jnp.mean(st * st, axis=-1, keepdims=True) + EPS)
    act[z] = swap_halves(st * scale * gain_ref[...], True).astype(BF)

    half_rows = own_rows // 2

    def ag_copy(way, k):
        to, block = (right, mod(z - k + 1, n_z)) if way == 0 else (left, mod(z + k - 1, n_z))
        ref = act.at[block] if k < half_z else act.at[block, pl.ds(way * half_rows, half_rows)]
        return pltpu.make_async_remote_copy(
            src_ref=ref, dst_ref=ref, send_sem=ag_send.at[way, k - 1], recv_sem=ag_recv.at[way, k - 1],
            device_id=to, device_id_type=MESH,
        )

    def ag_got(way, k):
        block = mod(z - k, n_z) if way == 0 else mod(z + k, n_z)
        ref = act.at[block] if k < half_z else act.at[block, pl.ds(way * half_rows, half_rows)]
        return pltpu.make_async_remote_copy(
            src_ref=ref, dst_ref=ref, send_sem=ag_send.at[way, k - 1], recv_sem=ag_recv.at[way, k - 1],
            device_id=right, device_id_type=MESH,
        )

    def ag_start(k):
        for way in range(2):
            ag_copy(way, k).start()

    def ag_next(k):
        for way in range(2):
            ag_got(way, k).wait_recv()
            if k < half_z:
                ag_copy(way, k + 1).start()

    def role(r):
        s = mod(x - z - r, n_x)
        return s, s * quads + zq < tiles

    x_to = {0: {"tp": mod(x + 1, n_x)}, 1: {"tp": mod(x - 1, n_x)}}
    mid = d_half // 2
    halves = (pl.ds(0, mid), pl.ds(mid, mid))

    def remote(ref, send, recv, to):
        return pltpu.make_async_remote_copy(
            src_ref=ref, dst_ref=ref, send_sem=send, recv_sem=recv, device_id=to, device_id_type=MESH
        )

    def xf_copy(m, way, s):
        return remote(w_at(c, all_rows, m, s), xf_send.at[m, way], xf_recv.at[m, way], x_to[way])

    def xh_copy(m, way, s):
        return remote(w_at(c, halves[way], m, s), xh_send.at[m, way], xh_recv.at[m, way], x_to[way])

    def p_copy(m, r, s):
        return remote(w_at(c, all_rows, m, s), p_send.at[m, r], p_recv.at[m, r], other)

    def x_owner(m):
        s, valid = role(0)

        @pl.when(valid)
        def _():
            remote(w_at(c, all_rows, m, s), st_send.at[m, 0], st_recv.at[m], right).wait_recv()
            xf_copy(m, 0, s).start()
            xf_copy(m, 1, s).start()
            p_copy(m, 0, s).start()

    def x_relay(m):
        for way, r in ((0, 1), (1, 3)):
            s, valid = role(r)

            @pl.when(valid)
            def _(way=way, r=r, s=s):
                xf_copy(m, way, s).wait_recv()
                xh_copy(m, way, s).start()
                p_copy(m, r, s).start()

    def x_last(m):
        s, valid = role(2)

        @pl.when(valid)
        def _():
            for way in range(2):
                xh_copy(m, way, s).wait_recv()
            p_copy(m, 2, s).start()

    def x_partner(m):
        for r in range(4):
            s, valid = role(r)

            @pl.when(valid)
            def _(r=r, s=s):
                remote(w_at(1 - c, all_rows, m, s), p_send.at[m, r], p_recv.at[m, r], other).wait_recv()

    meanwhile = [
        lambda: x_owner(0), lambda: x_owner(1),
        lambda: x_relay(0), lambda: x_owner(2), lambda: x_relay(1), lambda: x_last(0),
        lambda: x_relay(2), lambda: x_last(1), lambda: x_last(2),
        lambda: [x_partner(m) for m in range(3)],
    ]
    places = {1: (0, 1), 2: (2,), 3: (3, 4), 4: (5,), 5: (6, 7), 6: (), 7: (8,)}
    done = set()
    ag_start(1)
    for k in range(1, half_z + 1):
        ag_next(k)
        for at in places.get(k, ()):
            meanwhile[at]()
            done.add(at)
    for at in range(len(meanwhile)):
        if at not in done:
            meanwhile[at]()

    rbuf[0, 0, half_rows:, :] = jnp.zeros((own_rows - half_rows, d), BF)
    rbuf[1, 0, 0:half_rows, :] = jnp.zeros((half_rows, d), BF)

    def rs_copy(way, i, whole):
        rows = pl.ds(0, own_rows) if whole else pl.ds(way * half_rows, half_rows)
        return pltpu.make_async_remote_copy(
            src_ref=sbuf.at[way, i, rows], dst_ref=rbuf.at[way, i, rows],
            send_sem=rs_send.at[way, i], recv_sem=rs_recv.at[way, i],
            device_id=right if way == 0 else left, device_id_type=MESH,
        )

    def ring_step(i, unused):
        far = half_z - i
        one_at = mod(z + far, n_z)
        two_at = jnp.where(i == 0, z, mod(z - far, n_z))
        rows2 = jnp.concatenate([act[one_at], act[two_at]], axis=0)
        sums = dot(rows2[:, 0:d_half], w[0, :, 0 : 2 * ff_pad]) + dot(rows2[:, d_half:], w[1, :, 0 : 2 * ff_pad])
        gate, up = sums[:, 0:ff_pad], sums[:, ff_pad:]
        hidden = (gate / (1.0 + jnp.exp(-gate)) * up).astype(BF)
        part[:, 0:d_half] = dot_t(hidden, w[0, :, 2 * ff_pad :])
        part[:, d_half:] = dot_t(hidden, w[1, :, 2 * ff_pad :])

        @pl.when(i == 0)
        def _():
            own[...] = part[own_rows:, :]
            far_sum = part[0:own_rows, :].astype(BF)
            for way in range(2):
                sbuf[way, 0] = far_sum
                rs_copy(way, 0, False).start()

        @pl.when(i == 1)
        def _():
            for way in range(2):
                rs_copy(way, 0, False).wait_recv()

        @pl.when(i > 1)
        def _():
            for way in range(2):
                rs_copy(way, i - 1, True).wait_recv()

        @pl.when(i > 0)
        def _():
            for way in range(2):
                sbuf[way, i] = (rbuf[way, i - 1].astype(F32) + part[way * own_rows : (way + 1) * own_rows, :]).astype(BF)
                rs_copy(way, i, True).start()

        return unused

    lax.fori_loop(0, half_z, ring_step, 0)
    for way in range(2):
        rs_copy(way, half_z - 1, True).wait_recv()
    total = own[...] + rbuf[0, half_z - 1].astype(F32) + rbuf[1, half_z - 1].astype(F32)
    out_ref[...] = (stream[...] + swap_halves(total, False)).astype(out_ref.dtype)

    e_copy.wait_send()

    def g_sent(to, unused):
        g_copy(to).wait_send()
        return unused

    lax.fori_loop(z + 1, n_z, g_sent, 0)
    for m in range(3):

        def st_sent(j, unused, m=m):
            s, to = st_place(j)

            @pl.when(to != z)
            def _():
                st_copy(m, j, s, to).wait_send()

            return unused

        lax.fori_loop(0, tiles, st_sent, 0)
    for k in range(1, n_x):
        m_copy(k).wait_send()
    for way in range(2):
        for k in range(1, half_z + 1):
            ag_copy(way, k).wait_send()
        for i in range(half_z):
            rs_copy(way, i, i > 0).wait_send()
    for m in range(3):
        for r in range(4):
            s, valid = role(r)

            @pl.when(valid)
            def _(m=m, r=r, s=s):
                p_copy(m, r, s).wait_send()
                if r == 0:
                    xf_copy(m, 0, s).wait_send()
                    xf_copy(m, 1, s).wait_send()
                if r == 1:
                    xh_copy(m, 0, s).wait_send()
                if r == 3:
                    xh_copy(m, 1, s).wait_send()


def per_device(
    ssm_input, residual_in, log_step, decay_real, freq, in_real, in_imag, out_real, out_imag, skip,
    w_glu, b_glu, w_branch, norm_gain, w_gate, w_up, w_down,
):
    tok, width = ssm_input.shape
    groups, n_p = decay_real.shape
    group_size = in_real.shape[2]
    n_z, n_c, n_x = lax.axis_size("sp_0"), lax.axis_size("sp_1"), lax.axis_size("tp")
    d = residual_in.shape[1]
    wide = w_glu.shape[0]
    tiles = w_gate.shape[1] // LANES
    quads = n_z // n_x
    slots = -(-tiles // quads)
    assert n_c == 2 and n_x == 4 and slots < n_x and n_z % n_x == 0
    assert tok == SPAN * ROWS8 and 2 * n_p == LANES and w_gate.shape[1] % LANES == 0
    own_rows = tok // n_x
    n_state = groups * n_p
    half_z = n_z // 2
    vmem = pl.BlockSpec(memory_space=pltpu.VMEM)
    hbm = pl.BlockSpec(memory_space=pl.ANY)
    dma = pltpu.SemaphoreType.DMA
    return pl.pallas_call(
        functools.partial(kernel, (n_z, n_x, tiles, slots)),
        out_shape=jax.ShapeDtypeStruct((own_rows, d), BF),
        in_specs=[vmem] * 11 + [hbm] * 6,
        out_specs=vmem,
        scratch_shapes=[
            pltpu.VMEM((wide, wide), BF),
            pltpu.VMEM((wide, d), BF),
            pltpu.VMEM((own_rows, d), BF),
            pltpu.VMEM((2, d // 2, 3 * slots * LANES), BF),
            pltpu.VMEM((width, 2 * n_state), BF),
            pltpu.VMEM((width, 2 * n_state), BF),
            pltpu.VMEM((tok, 2 * n_state), F32),
            pltpu.VMEM((tok, 2 * n_state), BF),
            pltpu.VMEM((3, 2, n_state), F32),
            pltpu.VMEM((n_z, 2, n_state), F32),
            pltpu.VMEM((n_x, own_rows, width), BF),
            pltpu.VMEM((n_x, own_rows, width), BF),
            pltpu.VMEM((n_z, own_rows, d), BF),
            pltpu.VMEM((own_rows, d), F32),
            pltpu.VMEM((own_rows, d), F32),
            pltpu.VMEM((2 * own_rows, d), F32),
            pltpu.VMEM((2, half_z, own_rows, d), BF),
            pltpu.VMEM((2, half_z, own_rows, d), BF),
            dma((3,)), dma((3, tiles)), dma((3,)), dma((1,)), dma((1,)), dma((n_z,)), dma((n_z,)),
            dma((n_x,)), dma((n_x,)),
            dma((3, 2)), dma((3, 2)), dma((3, 2)), dma((3, 2)), dma((3, 4)), dma((3, 4)),
            dma((2, half_z)), dma((2, half_z)), dma((2, half_z)), dma((2, half_z)),
        ],
        compiler_params=pltpu.CompilerParams(collective_id=0, has_side_effects=True, vmem_limit_bytes=56 * 1024 * 1024),
        name="mixer_ffn",
    )(
        ssm_input,
        log_step.reshape(1, groups),
        decay_real,
        freq,
        in_real.transpose(0, 2, 1).reshape(groups * group_size, n_p),
        in_imag.transpose(0, 2, 1).reshape(groups * group_size, n_p),
        out_real.reshape(groups * group_size, n_p),
        out_imag.reshape(groups * group_size, n_p),
        skip.reshape(1, width),
        b_glu.reshape(1, wide),
        norm_gain.reshape(1, d),
        residual_in,
        w_glu,
        w_branch,
        w_gate,
        w_up,
        w_down.T,
    )


def solution(mesh):
    n_c = 2
    torus = Mesh(
        mesh.devices.reshape(mesh.shape["grp"], mesh.shape["sp"] // n_c, n_c, mesh.shape["tp"]),
        ("grp", "sp_0", "sp_1", "tp"),
    )
    in_specs = (
        P(GRP_SP, "tp"), P(GRP_SP, None), P("tp"), P("tp", None), P("tp", None),
        P("tp", None, None), P("tp", None, None), P("tp", None, None), P("tp", None, None), P("tp"),
        P(), P(), P(), P(), P(SP, "tp"), P(SP, "tp"), P("tp", SP),
    )
    return jax.shard_map(per_device, mesh=torus, in_specs=in_specs, out_specs=P(GRP_SP_TP, None), check_vma=False)
```

time: 210 us -> 149 us (0.71)
  Pallas kernels: 0 us -> 147 us
  blocking collectives: 81.3 us -> 0 us
  waiting for transfers between devices: 33.9 us -> 0 us
  other arithmetic: 28.9 us -> 0 us
  local copies, waits for them, and re-layouts: 24.7 us -> 1.57 us
  matrix products: 21.3 us -> 0 us
  between operations: 13.7 us -> 0.01 us
  starting transfers between devices: 4.57 us -> 0 us
    pallas_call x0 -> x1, Pallas kernels: none -> 147 us  [per_device(): pl.pallas_call(functools.partial(kernel, (n_z, n_x, tiles, slots)), out_s...]
    all_gather x2 -> x0, blocking collectives: 56.8 us -> none  [all_in_one(): both, at, found = (lax.all_gather(jnp.concatenate(lines), axis), 0, {})]
    all_gather x2 -> x0, waiting for transfers between devices: 27.5 us -> none  [the longest x1 27.5 us: per_device(): down_whole = lax.all_gather(w_down, SP, axis=1, tiled=True)]
    all_to_all x2 -> x0, blocking collectives: 24.5 us -> none  [the longest x1 14 us: summed_on_arrival(): lax.all_to_all(pieces, axis, split_axis=0, concat_axis=0, tiled=True)]
    dot_general x7 -> x0, matrix products: 21.3 us -> none  [the longest x1 7.42 us: per_device(): jnp.dot(hidden, down_whole, preferred_element_type=jnp.float32)]
    dynamic_update_slice x16 -> x0, local copies, waits for them, and re-layouts: 12.1 us -> none  [local_states(): lax.scan(carry_step, (zeros, zeros), (inner_re[:, -1], inner_im[:, -1]))]
    add x19 -> x0, other arithmetic: 8.78 us -> none  [the longest x1 6.71 us: per_device(): state_im = local_im + pow_re * carried[3][None] + pow_im * carried[2][None]]
    reduce_sum x2 -> x0, other arithmetic: 6.43 us -> none  [the longest x1 6.35 us: local_states(): jnp.sum(table_re[None] * block_im + table_im[None] * block_re, axis=2)]
  transfers between devices with their start and end apart: 3 -> 0, of which waited for: 2 -> 0; matrix products, arithmetic and copies ran while one was open for 31% -> 0% of each run, Pallas kernels for 0% -> 0%
where the time goes in v1:
time: 149 us
  Pallas kernels  147 us (99%)
  local copies, waits for them, and re-layouts  1.57 us (1%)
    pallas_call x1, Pallas kernels, per_device(): pl.pallas_call(functools.partial(kernel, (n_z, n_x, tiles, slots)), out_s...  147 us

profile of v1, /device:TPU:40, one launch (start us, length us, event | category | flops | bytes accessed | tf_op | source)
XLA Modules:
  0.0 148.7 jit_solution(16858293816009335796)
XLA Ops:
  0.0 147.1 %mixer_ffn.1 = bf16[32,2048]{1,0:T(8,128)(2,1)} custom-call(bf16[128,256]{1,0:T(8,128)(2,1)} %u_ref.1, f32[1,16]{1,0:T(1,128)} %bitcast.21, f32[16,64]{1,0:T(8,128)} %dr_ref.1, f32[16,64]{1,0:T(8,128)} %fq_ref.1, f32[256,64]{1,0:T(8,128)} %bitcast.14, f32[256,64]{1,0:T(8,128)} %bitcast.15, f32[256,64]{1,0:T(8,128)} %bitcast.16, f32[256,64]{1,0:T(8,128)} %bitcast.17, ...), custom_call_target="tpu_custom_call" | custom-call | tf_op jit(solution)/shard_map/mixer_ffn/pallas_call | solution.py:539
  147.1 1.6 %copy.19 = bf16[32,2048]{1,0:T(8,128)(2,1)} copy(bf16[32,2048]{1,0:T(8,128)(2,1)} %mixer_ffn.1) | data formatting | bytes 262144

commit v2 on v1

--- a/solution.py
+++ b/solution.py
@@ -15,6 +15,7 @@
 LANES = 128
 SPAN = 16
 ROWS8 = 8
+PARTS = 4
 BF = jnp.bfloat16
 F32 = jnp.float32
 MESH = pl.DeviceIdType.MESH
@@ -59,9 +60,9 @@
     u_ref, ls_ref, dr_ref, fq_ref, inr_ref, ini_ref, our_ref, oui_ref, skip_ref, bglu_ref, gain_ref,
     resid_hbm, wglu_hbm, wbr_hbm, wg_hbm, wu_hbm, wd_hbm,
     out_ref,
-    wglu, wbr, resid, w, tab_b, tab_c, drive, states, est, gst, mo, mrecv, act, stream, own, part, sbuf, rbuf,
-    cp_sem, st_send, st_recv, e_send, e_recv, g_send, g_recv, m_send, m_recv,
-    xf_send, xf_recv, xh_send, xh_recv, p_send, p_recv, ag_send, ag_recv, rs_send, rs_recv,
+    wglu, wbr, resid, packed, w, tab_b, tab_c, drive, states, est, gst, mo, mrecv, act, stream, own, part, sbuf, rbuf,
+    cp_sem, st_sent, st_recv, e_send, e_recv, g_send, g_recv, m_send, m_recv,
+    xf_send, xf_recv, xh_send, xh_recv, p_send, p_recv, ag_send, ag_recv, rs_send, rs_recv, pk_sem,
 ):
     n_z, n_x, tiles, slots = dims
     quads = n_z // n_x
@@ -96,6 +97,13 @@
     ]
     for copy in local:
         copy.start()
+    packs = []
+    for m, source in enumerate((wg_hbm, wu_hbm, wd_hbm)):
+        for j in range(tiles):
+            rows = pl.ds(m * d_block, d_block)
+            packs.append(pltpu.make_async_copy(source.at[:, pl.ds(j * LANES, LANES)], packed.at[j, rows, :], pk_sem.at[m, j]))
+    for copy in packs:
+        copy.start()
 
     diag = lax.broadcasted_iota(jnp.int32, (groups, groups), 0) == lax.broadcasted_iota(jnp.int32, (groups, groups), 1)
     step = jnp.sum(jnp.where(diag, jnp.broadcast_to(jnp.exp(ls_ref[...]), (groups, groups)), 0.0), axis=1, keepdims=True)
@@ -186,9 +194,7 @@
 
             @pl.when(s * quads + zq >= tiles)
             def _():
-                for m in range(3):
-                    at = (m * slots + s) * LANES
-                    w[:, :, at : at + LANES] = jnp.zeros((2, d_half, LANES), BF)
+                w[s] = jnp.zeros((2, n_z, 3 * d_block, LANES), BF)
 
     pl.semaphore_wait(barrier, n_z - 1 + n_x - 1 + 1)
 
@@ -217,42 +223,38 @@
 
     lax.fori_loop(z + 1, n_z, g_start, 0)
 
-    sources = (wg_hbm, wu_hbm, wd_hbm)
-
-    def w_at(core, rows, m, s):
-        return w.at[core, rows, pl.ds(pl.multiple_of((m * slots + s) * LANES, LANES), LANES)]
-
-    z_rows = pl.ds(pl.multiple_of(z * d_block, d_block), d_block)
-    all_rows = pl.ds(0, d_half)
-
-    def st_place(j):
-        s = lax.div(j, quads)
-        return s, lax.rem(j, quads) * n_x + mod(x - s, n_x)
-
-    def st_copy(m, j, s, to):
-        src = sources[m].at[:, pl.ds(pl.multiple_of(j * LANES, LANES), LANES)]
+    def tile_of(chip):
+        s = mod(x - chip, n_x)
+        return s, s * quads + lax.div(chip, n_x)
+
+    def st_copy(chip, s, j):
         return pltpu.make_async_remote_copy(
-            src_ref=src, dst_ref=w_at(c, z_rows, m, s), send_sem=st_send.at[m, j], recv_sem=st_recv.at[m],
-            device_id={"sp_0": to}, device_id_type=MESH,
+            src_ref=packed.at[j], dst_ref=w.at[s, c, z], send_sem=st_sent.at[chip], recv_sem=st_recv.at[z],
+            device_id={"sp_0": chip}, device_id_type=MESH,
         )
 
-    for m in range(3):
-
-        def st_start(j, unused, m=m):
-            s, to = st_place(j)
-
-            @pl.when(to != z)
-            def _():
-                st_copy(m, j, s, to).start()
-
-            @pl.when(to == z)
-            def _():
-                src = sources[m].at[:, pl.ds(pl.multiple_of(j * LANES, LANES), LANES)]
-                pltpu.make_async_copy(src, w_at(c, z_rows, m, s), st_recv.at[m]).start()
-
-            return unused
-
-        lax.fori_loop(0, tiles, st_start, 0)
+    def st_chip(k):
+        up = half_z - lax.div(k, 2)
+        return mod(jnp.where(lax.rem(k, 2) == 0, z + up, z - up + 1), n_z)
+
+    def st_start(k, unused):
+        chip = st_chip(k)
+        s, j = tile_of(chip)
+
+        @pl.when(j < tiles)
+        def _():
+            st_copy(chip, s, j).start()
+
+        return unused
+
+    for copy in packs:
+        copy.wait()
+    lax.fori_loop(0, n_z - 1, st_start, 0)
+    s_mine, j_mine = tile_of(z)
+
+    @pl.when(j_mine < tiles)
+    def _():
+        w[s_mine, c, z] = packed[j_mine]
 
     def add_state(frm, carry):
         g_got = pltpu.make_async_remote_copy(
@@ -316,130 +318,142 @@
 
     half_rows = own_rows // 2
 
-    def ag_copy(way, k):
-        to, block = (right, mod(z - k + 1, n_z)) if way == 0 else (left, mod(z + k - 1, n_z))
-        ref = act.at[block] if k < half_z else act.at[block, pl.ds(way * half_rows, half_rows)]
-        return pltpu.make_async_remote_copy(
-            src_ref=ref, dst_ref=ref, send_sem=ag_send.at[way, k - 1], recv_sem=ag_recv.at[way, k - 1],
-            device_id=to, device_id_type=MESH,
-        )
-
-    def ag_got(way, k):
-        block = mod(z - k, n_z) if way == 0 else mod(z + k, n_z)
-        ref = act.at[block] if k < half_z else act.at[block, pl.ds(way * half_rows, half_rows)]
-        return pltpu.make_async_remote_copy(
-            src_ref=ref, dst_ref=ref, send_sem=ag_send.at[way, k - 1], recv_sem=ag_recv.at[way, k - 1],
-            device_id=right, device_id_type=MESH,
-        )
-
-    def ag_start(k):
-        for way in range(2):
-            ag_copy(way, k).start()
-
-    def ag_next(k):
-        for way in range(2):
-            ag_got(way, k).wait_recv()
-            if k < half_z:
-                ag_copy(way, k + 1).start()
-
-    def role(r):
-        s = mod(x - z - r, n_x)
-        return s, s * quads + zq < tiles
-
-    x_to = {0: {"tp": mod(x + 1, n_x)}, 1: {"tp": mod(x - 1, n_x)}}
-    mid = d_half // 2
-    halves = (pl.ds(0, mid), pl.ds(mid, mid))
+    wide_part = d // PARTS
 
     def remote(ref, send, recv, to):
         return pltpu.make_async_remote_copy(
             src_ref=ref, dst_ref=ref, send_sem=send, recv_sem=recv, device_id=to, device_id_type=MESH
         )
 
-    def xf_copy(m, way, s):
-        return remote(w_at(c, all_rows, m, s), xf_send.at[m, way], xf_recv.at[m, way], x_to[way])
-
-    def xh_copy(m, way, s):
-        return remote(w_at(c, halves[way], m, s), xh_send.at[m, way], xh_recv.at[m, way], x_to[way])
-
-    def p_copy(m, r, s):
-        return remote(w_at(c, all_rows, m, s), p_send.at[m, r], p_recv.at[m, r], other)
-
-    def x_owner(m):
+    def ag_ref(way, k, q, block):
+        rows = pl.ds(0, own_rows) if k < half_z else pl.ds(way * half_rows, half_rows)
+        return act.at[block, rows, pl.ds(q * wide_part, wide_part)]
+
+    def ag_copy(way, k, q):
+        to, block = (right, mod(z - k + 1, n_z)) if way == 0 else (left, mod(z + k - 1, n_z))
+        return remote(ag_ref(way, k, q, block), ag_send.at[way, k - 1, q], ag_recv.at[way, k - 1, q], to)
+
+    def ag_got(way, k, q):
+        block = mod(z - k, n_z) if way == 0 else mod(z + k, n_z)
+        return remote(ag_ref(way, k, q, block), ag_send.at[way, k - 1, q], ag_recv.at[way, k - 1, q], right)
+
+    def ag_start(k):
+        for q in range(PARTS):
+            for way in range(2):
+                ag_copy(way, k, q).start()
+
+    def ag_next(k):
+        for q in range(PARTS):
+            for way in range(2):
+                ag_got(way, k, q).wait_recv()
+                if k < half_z:
+                    ag_copy(way, k + 1, q).start()
+
+    def role(r):
+        s = mod(x - z - r, n_x)
+        return s, s * quads + zq < tiles
+
+    x_to = {0: {"tp": mod(x + 1, n_x)}, 1: {"tp": mod(x - 1, n_x)}}
+    fours = n_z // 4
+
+    def group(core, s, g):
+        return w.at[s, core, pl.ds(g * fours, fours)]
+
+    def xf_copy(g, way, s):
+        return remote(group(c, s, g), xf_send.at[g, way], xf_recv.at[g, way], x_to[way])
+
+    def xh_copy(g, s):
+        return remote(group(c, s, g), xh_send.at[g], xh_recv.at[g], x_to[g // 2])
+
+    def p_copy(g, r, s):
+        return remote(group(c, s, g), p_send.at[g, r], p_recv.at[g, r], other)
+
+    def x_owner(g):
         s, valid = role(0)
 
         @pl.when(valid)
         def _():
-            remote(w_at(c, all_rows, m, s), st_send.at[m, 0], st_recv.at[m], right).wait_recv()
-            xf_copy(m, 0, s).start()
-            xf_copy(m, 1, s).start()
-            p_copy(m, 0, s).start()
-
-    def x_relay(m):
+            for chip in range(g * fours, (g + 1) * fours):
+
+                @pl.when(z != chip)
+                def _(chip=chip):
+                    remote(w.at[s, c, chip], st_sent.at[chip], st_recv.at[chip], right).wait_recv()
+
+            for way in range(2):
+                xf_copy(g, way, s).start()
+            p_copy(g, 0, s).start()
+
+    def x_relay(g):
         for way, r in ((0, 1), (1, 3)):
             s, valid = role(r)
 
             @pl.when(valid)
             def _(way=way, r=r, s=s):
-                xf_copy(m, way, s).wait_recv()
-                xh_copy(m, way, s).start()
-                p_copy(m, r, s).start()
-
-    def x_last(m):
+                xf_copy(g, way, s).wait_recv()
+                if g // 2 == way:
+                    xh_copy(g, s).start()
+                p_copy(g, r, s).start()
+
+    def x_last(g):
         s, valid = role(2)
 
         @pl.when(valid)
         def _():
-            for way in range(2):
-                xh_copy(m, way, s).wait_recv()
-            p_copy(m, 2, s).start()
-
-    def x_partner(m):
+            xh_copy(g, s).wait_recv()
+            p_copy(g, 2, s).start()
+
+    def x_partner(g):
         for r in range(4):
             s, valid = role(r)
 
             @pl.when(valid)
             def _(r=r, s=s):
-                remote(w_at(1 - c, all_rows, m, s), p_send.at[m, r], p_recv.at[m, r], other).wait_recv()
-
-    meanwhile = [
-        lambda: x_owner(0), lambda: x_owner(1),
-        lambda: x_relay(0), lambda: x_owner(2), lambda: x_relay(1), lambda: x_last(0),
-        lambda: x_relay(2), lambda: x_last(1), lambda: x_last(2),
-        lambda: [x_partner(m) for m in range(3)],
-    ]
-    places = {1: (0, 1), 2: (2,), 3: (3, 4), 4: (5,), 5: (6, 7), 6: (), 7: (8,)}
-    done = set()
+                remote(group(1 - c, s, g), p_send.at[g, r], p_recv.at[g, r], other).wait_recv()
+
     ag_start(1)
-    for k in range(1, half_z + 1):
-        ag_next(k)
-        for at in places.get(k, ()):
-            meanwhile[at]()
-            done.add(at)
-    for at in range(len(meanwhile)):
-        if at not in done:
-            meanwhile[at]()
+    after = {
+        0: [(x_owner, 0), (x_owner, 1)],
+        1: [(x_owner, 2)],
+        2: [(x_owner, 3)],
+        3: [(x_relay, 0)],
+        4: [(x_relay, 1)],
+        5: [(x_relay, 2), (x_last, 0)],
+        6: [(x_relay, 3), (x_last, 1)],
+        7: [(x_last, 2)],
+        8: [(x_last, 3)] + [(x_partner, g) for g in range(4)],
+    }
+    for k in range(half_z + 1):
+        if k:
+            ag_next(k)
+        for what, g in after.get(k, ()):
+            what(g)
 
     rbuf[0, 0, half_rows:, :] = jnp.zeros((own_rows - half_rows, d), BF)
     rbuf[1, 0, 0:half_rows, :] = jnp.zeros((half_rows, d), BF)
 
-    def rs_copy(way, i, whole):
+    def rs_copy(way, i, q, whole):
         rows = pl.ds(0, own_rows) if whole else pl.ds(way * half_rows, half_rows)
+        lanes = pl.ds(q * wide_part, wide_part)
         return pltpu.make_async_remote_copy(
-            src_ref=sbuf.at[way, i, rows], dst_ref=rbuf.at[way, i, rows],
-            send_sem=rs_send.at[way, i], recv_sem=rs_recv.at[way, i],
+            src_ref=sbuf.at[way, i, rows, lanes], dst_ref=rbuf.at[way, i, rows, lanes],
+            send_sem=rs_send.at[way, i, q], recv_sem=rs_recv.at[way, i, q],
             device_id=right if way == 0 else left, device_id_type=MESH,
         )
+
+    def matrix(core, kinds):
+        at = [(m * d_block, s) for m in kinds for s in range(slots)]
+        return jnp.concatenate([w[s, core, :, r : r + d_block, :].reshape(d_half, LANES) for r, s in at], axis=1)
 
     def ring_step(i, unused):
         far = half_z - i
         one_at = mod(z + far, n_z)
         two_at = jnp.where(i == 0, z, mod(z - far, n_z))
         rows2 = jnp.concatenate([act[one_at], act[two_at]], axis=0)
-        sums = dot(rows2[:, 0:d_half], w[0, :, 0 : 2 * ff_pad]) + dot(rows2[:, d_half:], w[1, :, 0 : 2 * ff_pad])
+        sums = dot(rows2[:, 0:d_half], matrix(0, (0, 1))) + dot(rows2[:, d_half:], matrix(1, (0, 1)))
         gate, up = sums[:, 0:ff_pad], sums[:, ff_pad:]
         hidden = (gate / (1.0 + jnp.exp(-gate)) * up).astype(BF)
-        part[:, 0:d_half] = dot_t(hidden, w[0, :, 2 * ff_pad :])
-        part[:, d_half:] = dot_t(hidden, w[1, :, 2 * ff_pad :])
+        part[:, 0:d_half] = dot_t(hidden, matrix(0, (2,)))
+        part[:, d_half:] = dot_t(hidden, matrix(1, (2,)))
 
         @pl.when(i == 0)
         def _():
@@ -447,29 +461,33 @@
             far_sum = part[0:own_rows, :].astype(BF)
             for way in range(2):
                 sbuf[way, 0] = far_sum
-                rs_copy(way, 0, False).start()
+            for q in range(PARTS):
+                for way in range(2):
+                    rs_copy(way, 0, q, False).start()
+
+        def pass_on(i, whole):
+            for q in range(PARTS):
+                lanes = slice(q * wide_part, (q + 1) * wide_part)
+                for way in range(2):
+                    rs_copy(way, i - 1, q, whole).wait_recv()
+                    mine = part[way * own_rows : (way + 1) * own_rows, lanes]
+                    sbuf[way, i, :, lanes] = (rbuf[way, i - 1, :, lanes].astype(F32) + mine).astype(BF)
+                    rs_copy(way, i, q, True).start()
 
         @pl.when(i == 1)
         def _():
-            for way in range(2):
-                rs_copy(way, 0, False).wait_recv()
+            pass_on(1, False)
 
         @pl.when(i > 1)
         def _():
-            for way in range(2):
-                rs_copy(way, i - 1, True).wait_recv()
-
-        @pl.when(i > 0)
-        def _():
-            for way in range(2):
-                sbuf[way, i] = (rbuf[way, i - 1].astype(F32) + part[way * own_rows : (way + 1) * own_rows, :]).astype(BF)
-                rs_copy(way, i, True).start()
+            pass_on(i, True)
 
         return unused
 
     lax.fori_loop(0, half_z, ring_step, 0)
     for way in range(2):
-        rs_copy(way, half_z - 1, True).wait_recv()
+        for q in range(PARTS):
+            rs_copy(way, half_z - 1, q, True).wait_recv()
     total = own[...] + rbuf[0, half_z - 1].astype(F32) + rbuf[1, half_z - 1].astype(F32)
     out_ref[...] = (stream[...] + swap_halves(total, False)).astype(out_ref.dtype)
 
@@ -480,39 +498,39 @@
         return unused
 
     lax.fori_loop(z + 1, n_z, g_sent, 0)
-    for m in range(3):
-
-        def st_sent(j, unused, m=m):
-            s, to = st_place(j)
-
-            @pl.when(to != z)
-            def _():
-                st_copy(m, j, s, to).wait_send()
-
-            return unused
-
-        lax.fori_loop(0, tiles, st_sent, 0)
+
+    def st_left(k, unused):
+        chip = st_chip(k)
+        s, j = tile_of(chip)
+
+        @pl.when(j < tiles)
+        def _():
+            st_copy(chip, s, j).wait_send()
+
+        return unused
+
+    lax.fori_loop(0, n_z - 1, st_left, 0)
     for k in range(1, n_x):
         m_copy(k).wait_send()
     for way in range(2):
         for k in range(1, half_z + 1):
-            ag_copy(way, k).wait_send()
+            for q in range(PARTS):
+                ag_copy(way, k, q).wait_send()
         for i in range(half_z):
-            rs_copy(way, i, i > 0).wait_send()
-    for m in range(3):
+            for q in range(PARTS):
+                rs_copy(way, i, q, i > 0).wait_send()
+    for g in range(4):
         for r in range(4):
             s, valid = role(r)
 
             @pl.when(valid)
-            def _(m=m, r=r, s=s):
-                p_copy(m, r, s).wait_send()
+            def _(g=g, r=r, s=s):
+                p_copy(g, r, s).wait_send()
                 if r == 0:
-                    xf_copy(m, 0, s).wait_send()
-                    xf_copy(m, 1, s).wait_send()
-                if r == 1:
-                    xh_copy(m, 0, s).wait_send()
-                if r == 3:
-                    xh_copy(m, 1, s).wait_send()
+                    xf_copy(g, 0, s).wait_send()
+                    xf_copy(g, 1, s).wait_send()
+                if (r, g // 2) in ((1, 0), (3, 1)):
+                    xh_copy(g, s).wait_send()
 
 
 def per_device(
@@ -545,7 +563,8 @@
             pltpu.VMEM((wide, wide), BF),
             pltpu.VMEM((wide, d), BF),
             pltpu.VMEM((own_rows, d), BF),
-            pltpu.VMEM((2, d // 2, 3 * slots * LANES), BF),
+            pltpu.VMEM((tiles, 3 * w_gate.shape[0], LANES), BF),
+            pltpu.VMEM((slots, 2, n_z, 3 * w_gate.shape[0], LANES), BF),
             pltpu.VMEM((width, 2 * n_state), BF),
             pltpu.VMEM((width, 2 * n_state), BF),
             pltpu.VMEM((tok, 2 * n_state), F32),
@@ -560,10 +579,11 @@
             pltpu.VMEM((2 * own_rows, d), F32),
             pltpu.VMEM((2, half_z, own_rows, d), BF),
             pltpu.VMEM((2, half_z, own_rows, d), BF),
-            dma((3,)), dma((3, tiles)), dma((3,)), dma((1,)), dma((1,)), dma((n_z,)), dma((n_z,)),
+            dma((3,)), dma((n_z,)), dma((n_z,)), dma((1,)), dma((1,)), dma((n_z,)), dma((n_z,)),
             dma((n_x,)), dma((n_x,)),
-            dma((3, 2)), dma((3, 2)), dma((3, 2)), dma((3, 2)), dma((3, 4)), dma((3, 4)),
-            dma((2, half_z)), dma((2, half_z)), dma((2, half_z)), dma((2, half_z)),
+            dma((4, 2)), dma((4, 2)), dma((4,)), dma((4,)), dma((4, 4)), dma((4, 4)),
+            dma((2, half_z, PARTS)), dma((2, half_z, PARTS)), dma((2, half_z, PARTS)), dma((2, half_z, PARTS)),
+            dma((3, tiles)),
         ],
         compiler_params=pltpu.CompilerParams(collective_id=0, has_side_effects=True, vmem_limit_bytes=56 * 1024 * 1024),
         name="mixer_ffn",

time: 149 us -> 134 us (0.90)
  Pallas kernels: 147 us -> 133 us
    pallas_call x1, Pallas kernels: 147 us -> 133 us  [per_device(): pl.pallas_call(functools.partial(kernel, (n_z, n_x, tiles, slots)), out_s...]
where the time goes in v2:
time: 134 us
  Pallas kernels  133 us (99%)
  local copies, waits for them, and re-layouts  1.57 us (1%)
    pallas_call x1, Pallas kernels, per_device(): pl.pallas_call(functools.partial(kernel, (n_z, n_x, tiles, slots)), out_s...  133 us

profile of v2, /device:TPU:40, one launch (start us, length us, event | category | flops | bytes accessed | tf_op | source)
XLA Modules:
  0.0 134.1 jit_solution(15776542298227045875)
XLA Ops:
  0.0 132.5 %mixer_ffn.1 = bf16[32,2048]{1,0:T(8,128)(2,1)} custom-call(bf16[128,256]{1,0:T(8,128)(2,1)} %u_ref.1, f32[1,16]{1,0:T(1,128)} %bitcast.21, f32[16,64]{1,0:T(8,128)} %dr_ref.1, f32[16,64]{1,0:T(8,128)} %fq_ref.1, f32[256,64]{1,0:T(8,128)} %bitcast.14, f32[256,64]{1,0:T(8,128)} %bitcast.15, f32[256,64]{1,0:T(8,128)} %bitcast.16, f32[256,64]{1,0:T(8,128)} %bitcast.17, ...), custom_call_target="tpu_custom_call" | custom-call | tf_op jit(solution)/shard_map/mixer_ffn/pallas_call | solution.py:557
  132.5 1.6 %copy.19 = bf16[32,2048]{1,0:T(8,128)(2,1)} copy(bf16[32,2048]{1,0:T(8,128)(2,1)} %mixer_ffn.1) | data formatting | bytes 262144

commit v3 on v2

--- a/solution.py
+++ b/solution.py
@@ -135,7 +135,6 @@
     keep = lax.div(row, group_size) == lax.div(lane, lanes_state)
 
     tab_b[...] = jnp.zeros_like(tab_b)
-    tab_c[...] = jnp.zeros_like(tab_c)
 
     def put(table, k, col, value):
         table[k * pair_rows : (k + 1) * pair_rows, col + k * LANES : col + (k + 1) * LANES] = jnp.where(keep, value, 0.0).astype(BF)
@@ -149,8 +148,6 @@
         ir, ii = twice_of(inr_ref, k), twice_of(ini_ref, k)
         put(tab_b, k, 0, hr * ir - hi * ii)
         put(tab_b, k, n_state, hr * ii + hi * ir)
-        put(tab_c, k, 0, twice_of(our_ref, k))
-        put(tab_c, k, n_state, -twice_of(oui_ref, k))
 
     to_row = lax.broadcasted_iota(jnp.int32, (tok, tok), 0)
     to_col = lax.broadcasted_iota(jnp.int32, (tok, tok), 1)
@@ -234,8 +231,8 @@
         )
 
     def st_chip(k):
-        up = half_z - lax.div(k, 2)
-        return mod(jnp.where(lax.rem(k, 2) == 0, z + up, z - up + 1), n_z)
+        up = lax.div(k, 2) + 1
+        return mod(jnp.where(lax.rem(k, 2) == 0, z + up, z - up), n_z)
 
     def st_start(k, unused):
         chip = st_chip(k)
@@ -255,6 +252,11 @@
     @pl.when(j_mine < tiles)
     def _():
         w[s_mine, c, z] = packed[j_mine]
+
+    tab_c[...] = jnp.zeros_like(tab_c)
+    for k in range(n_state // LANES):
+        put(tab_c, k, 0, twice_of(our_ref, k))
+        put(tab_c, k, n_state, -twice_of(oui_ref, k))
 
     def add_state(frm, carry):
         g_got = pltpu.make_async_remote_copy(

time: 134 us -> 133 us (level)
  no operation moved by 1% of the time
where the time goes in v3:
time: 133 us
  Pallas kernels  132 us (99%)
  local copies, waits for them, and re-layouts  1.57 us (1%)
    pallas_call x1, Pallas kernels, per_device(): pl.pallas_call(functools.partial(kernel, (n_z, n_x, tiles, slots)), out_s...  132 us

profile of v3, /device:TPU:40, one launch (start us, length us, event | category | flops | bytes accessed | tf_op | source)
XLA Modules:
  0.0 133.2 jit_solution(15614240093554208736)
XLA Ops:
  0.0 131.6 %mixer_ffn.1 = bf16[32,2048]{1,0:T(8,128)(2,1)} custom-call(bf16[128,256]{1,0:T(8,128)(2,1)} %u_ref.1, f32[1,16]{1,0:T(1,128)} %bitcast.21, f32[16,64]{1,0:T(8,128)} %dr_ref.1, f32[16,64]{1,0:T(8,128)} %fq_ref.1, f32[256,64]{1,0:T(8,128)} %bitcast.14, f32[256,64]{1,0:T(8,128)} %bitcast.15, f32[256,64]{1,0:T(8,128)} %bitcast.16, f32[256,64]{1,0:T(8,128)} %bitcast.17, ...), custom_call_target="tpu_custom_call" | custom-call | tf_op jit(solution)/shard_map/mixer_ffn/pallas_call | solution.py:559
  131.6 1.6 %copy.19 = bf16[32,2048]{1,0:T(8,128)(2,1)} copy(bf16[32,2048]{1,0:T(8,128)(2,1)} %mixer_ffn.1) | data formatting | bytes 262144
